TPU v7x, 32 devices: a whole 2x2x4 slice. The times are simulated.
32 devices in a mesh: ep: 8 (over z, x), tp: 4 (over y, core).
Axes of the slice: x: 2, y: 2, z: 4, core: 2. Of those that a mesh axis runs over, the one named last changes fastest.
Arguments:
- recurrence_query: bfloat16 [1024, 1024], P('ep', 'tp'), may hold values from -6 to 6
- forget_preactivation: bfloat16 [1024, 1024], P('ep', 'tp'), may hold values from -7 to 7
- recurrence_value: bfloat16 [1024, 1024], P('ep', 'tp'), may hold values from -6 to 6
- output_gate_preactivation: bfloat16 [1024, 1024], P('ep', 'tp'), may hold values from -6 to 6
- forget_margin: float32 [1024], P('tp'), may hold values from 0 to 0.1
- surge_log_decay: float32 [8, 1024], P('tp', 'ep'), may hold values from -1.4 to 0
- head_norm_gain: float32 [1024], P('tp'), may hold values from 0.1 to 1.9
- recurrence_output_matrix: bfloat16 [1024, 4096], P('tp'), may hold values from -0.1875 to 0.1875
- second_micro_input: bfloat16 [1024, 4096], P(('ep', 'tp')), may hold values from -6 to 6
- expert_norm_gain: float32 [4096], replicated, may hold values from 0.1 to 1.9
- routes: int32 [1024, 2], P('ep'), may hold values from 0 to 7, all different within a row; in each aligned block of 32 rows (0 to 31, 32 to 63, ...) at most 16 rows name the same one
- router_chosen_logits: float32 [1024, 2], P(('ep', 'tp')), may hold values from -6 to 6
- expert_gate_matrix: bfloat16 [8, 4096, 1408], P('ep', None, 'tp'), may hold values from -0.09375 to 0.09375
- expert_up_matrix: bfloat16 [8, 4096, 1408], P('ep', None, 'tp'), may hold values from -0.09375 to 0.09375
- expert_down_matrix: bfloat16 [8, 1408, 4096], P('ep', 'tp'), may hold values from -0.15625 to 0.15625
Outputs:
- mixed: bfloat16 [1024, 4096], P(('ep', 'tp'))
- moe_out: bfloat16 [1024, 4096], P(('ep', 'tp'))
Inputs may be any that keep to these rules, and one draw needn't show every extreme that they name: `routes`: in the rows of one device (aligned blocks of 32 rows) no expert is named more than 16 times, and the experts of a row differ.
All inputs are finite; a program needn't handle non-finite values.
Results may differ from a plain program's by a relative error of at most 0.019.
Values may be sent and summed in bfloat16 or wider, within the bound.
A program may use at most 128 MiB of HBM per device.

v0:
```python
import jax
import jax.numpy as jnp
from jax import lax
from jax.sharding import PartitionSpec as P

TOP = 2
SPAN = 64


epsilon = 1e-06
highest = lax.Precision.HIGHEST


def entering_2(value, axis, combine, identity):
    size, mine = (lax.axis_size(axis), lax.axis_index(axis))
    everything = jax.tree.map(
        lambda part, kind: lax.all_gather(part.astype(kind), axis),
        value,
        (jnp.bfloat16, jnp.bfloat16),
    )
    start = jax.tree.map(
        lambda part, zero: jnp.broadcast_to(jnp.asarray(zero, part.dtype), part.shape),
        value,
        identity,
    )

    def hop(k, before):
        reached = k < mine
        new = combine(
            before, jax.tree.map(lambda part, own: part[k].astype(own.dtype), everything, value)
        )
        return jax.tree.map(lambda a, b: jnp.where(reached, a, b), new, before)

    return lax.fori_loop(0, size, hop, start)


def span_recurrence(query, inflow, decay_logarithm, values):
    number_of_heads, seq_len, key_width = query.shape
    span_count = seq_len // SPAN

    def to_spans(array):
        return array.reshape(number_of_heads, span_count, SPAN, array.shape[-1]).transpose(
            1, 0, 2, 3
        )

    lower_mask = jnp.tril(jnp.ones((SPAN, SPAN), bool))

    def advance(carried, inputs):
        query_span, inflow_span, decay_span, value_span = inputs
        running = jnp.cumsum(decay_span, axis=1)
        lifted_query = query_span * jnp.exp(running)
        lowered_inflow = inflow_span * jnp.exp(-running)
        scores = jnp.einsum("htd,hsd->hts", lifted_query, lowered_inflow, precision=highest)
        scores = jnp.where(lower_mask[None, :, :], scores, 0.0)
        output = jnp.einsum("hts,hsv->htv", scores, value_span, precision=highest)
        output = output + jnp.einsum("htd,hdv->htv", lifted_query, carried, precision=highest)
        closing = running[:, -1:, :]
        updated = jnp.exp(closing[:, 0, :])[:, :, None] * carried + jnp.einsum(
            "hsd,hsv->hdv", inflow_span * jnp.exp(closing - running), value_span, precision=highest
        )
        return (updated, output)

    start_state = jnp.zeros((number_of_heads, key_width, values.shape[-1]), jnp.float32)
    final_state, outputs = lax.scan(
        advance,
        start_state,
        (to_spans(query), to_spans(inflow), to_spans(decay_logarithm), to_spans(values)),
    )
    return (
        final_state,
        outputs.transpose(1, 0, 2, 3).reshape(number_of_heads, seq_len, values.shape[-1]),
    )


def chain_states(earlier, later):
    return (earlier[0] + later[0], jnp.exp(later[0])[:, :, None] * earlier[1] + later[1])


def slot_positions(block_routes, expert_count):
    chosen = block_routes.reshape(-1)
    table = (chosen[:, None] == jnp.arange(expert_count, dtype=jnp.int32)[None, :]).astype(
        jnp.int32
    )
    before = jnp.cumsum(table, axis=0) - table
    return (chosen, jnp.sum(before * table, axis=1))


def expert_hidden(flat_rows, gate_local, up_local):
    gate_proj = jnp.dot(flat_rows, gate_local, preferred_element_type=jnp.float32)
    up_proj = jnp.dot(flat_rows, up_local, preferred_element_type=jnp.float32)
    return (jax.nn.silu(gate_proj) * up_proj).astype(jnp.bfloat16)


def per_device(
    recurrence_query,
    forget_preactivation,
    recurrence_value,
    output_gate_preactivation,
    forget_margin,
    surge_log_decay,
    head_norm_gain,
    recurrence_output_matrix,
    second_micro_input,
    expert_norm_gain,
    routes,
    router_chosen_logits,
    expert_gate_matrix,
    expert_up_matrix,
    expert_down_matrix,
):
    number_of_heads = surge_log_decay.shape[0]
    seq_len = recurrence_query.shape[0]

    def heads_leading(array):
        return array.astype(jnp.float32).reshape(seq_len, number_of_heads, -1).transpose(1, 0, 2)

    closed_flag = jax.nn.sigmoid(-forget_preactivation.astype(jnp.float32)) * forget_margin
    decay_logarithm = heads_leading(jnp.log1p(-closed_flag)) + surge_log_decay[:, :, None]
    query = heads_leading(recurrence_query)
    final_state, local_out = span_recurrence(
        query, heads_leading(closed_flag), decay_logarithm, heads_leading(recurrence_value)
    )
    running = jnp.cumsum(decay_logarithm, axis=1)
    totals = running[:, -1, :]
    entering = entering_2(
        (totals, final_state),
        "ep",
        chain_states,
        (jnp.zeros_like(totals), jnp.zeros_like(final_state)),
    )
    output = local_out + jnp.einsum(
        "htd,hdv->htv", query * jnp.exp(running), entering[1], precision=highest
    )
    output = output * lax.rsqrt(jnp.mean(output * output, axis=-1, keepdims=True) + epsilon)
    output = output.transpose(1, 0, 2).reshape(seq_len, -1)
    hidden_a = (
        output * head_norm_gain * jax.nn.silu(output_gate_preactivation.astype(jnp.float32))
    ).astype(jnp.bfloat16)
    tp_count = lax.axis_size("tp")
    tp_rank = lax.axis_index("tp")
    expert_count = lax.axis_size("ep")
    tok_rows = second_micro_input.shape[0]
    width = second_micro_input.shape[1]
    capacity = 2 * tok_rows * TOP // expert_count
    moe_rows = second_micro_input.astype(jnp.float32)
    normed = (
        moe_rows
        * lax.rsqrt(jnp.mean(moe_rows * moe_rows, axis=-1, keepdims=True) + epsilon)
        * expert_norm_gain
    ).astype(jnp.bfloat16)
    own_routes = lax.dynamic_slice_in_dim(routes, tp_rank * tok_rows, tok_rows, 0)
    own_chosen, own_places = slot_positions(own_routes, expert_count)
    copy_source = jnp.arange(tok_rows * TOP, dtype=jnp.int32) // TOP
    gate_local = expert_gate_matrix[0]
    up_local = expert_up_matrix[0]
    down_local = expert_down_matrix[0]
    hidden_width = gate_local.shape[1]
    buffer = jnp.zeros((expert_count * capacity, width), jnp.bfloat16)
    buffer = buffer.at[own_chosen * capacity + own_places].set(normed[copy_source])
    arrived = lax.all_to_all(
        buffer.reshape(expert_count, capacity, width), "ep", split_axis=0, concat_axis=0, tiled=True
    )
    piece = lax.all_gather(arrived, "tp", axis=0, tiled=True)
    piece_count = piece.shape[0]
    slot_count = piece.shape[1]
    produced = expert_hidden(piece.reshape(piece_count * slot_count, width), gate_local, up_local)
    hidden_b = produced.reshape(piece_count, slot_count, hidden_width)
    hidden_b = hidden_b.reshape(tp_count, expert_count * capacity, hidden_width)
    mix_rows = seq_len // tp_count
    expert_slots = expert_count * capacity
    per_block = mix_rows + expert_slots
    first_block = jnp.int32(0) // per_block
    pieces = []
    for offset in range(per_block * lax.axis_size("tp") // per_block):
        block_index = first_block + offset
        mix_part = lax.dynamic_slice_in_dim(hidden_a, block_index * mix_rows, mix_rows, 0)
        expert_part = lax.dynamic_index_in_dim(hidden_b, block_index, 0, keepdims=False)
        pieces.append(
            jnp.dot(mix_part, recurrence_output_matrix, preferred_element_type=jnp.float32)
        )
        pieces.append(jnp.dot(expert_part, down_local, preferred_element_type=jnp.float32))
    summed = lax.psum_scatter(
        jnp.concatenate(pieces, axis=0).astype(jnp.bfloat16), "tp", scatter_dimension=0, tiled=True
    ).astype(jnp.float32)
    mixed = summed[:mix_rows].astype(jnp.bfloat16)
    expert_rows = summed[mix_rows:].astype(jnp.bfloat16)
    returned = lax.all_to_all(
        expert_rows.reshape(expert_count, capacity, width),
        "ep",
        split_axis=0,
        concat_axis=0,
        tiled=True,
    )
    picked = returned.reshape(expert_count * capacity, width)[own_chosen * capacity + own_places]
    route_weight = jax.nn.softmax(router_chosen_logits, axis=-1)
    moe_out = jnp.sum(
        route_weight[:, :, None] * picked.reshape(tok_rows, TOP, width).astype(jnp.float32), axis=1
    )
    return (mixed, moe_out.astype(jnp.bfloat16))


def solution(mesh):
    return jax.shard_map(
        per_device,
        mesh=mesh,
        in_specs=(
            P("ep", "tp"),
            P("ep", "tp"),
            P("ep", "tp"),
            P("ep", "tp"),
            P("tp"),
            P("tp", "ep"),
            P("tp"),
            P("tp", None),
            P(("ep", "tp"), None),
            P(),
            P("ep", None),
            P(("ep", "tp"), None),
            P("ep", None, "tp"),
            P("ep", None, "tp"),
            P("ep", "tp", None),
        ),
        out_specs=(P(("ep", "tp"), None), P(("ep", "tp"), None)),
        check_vma=False,
    )
```

profile of v0, /device:TPU:0, one launch (start us, length us, event | category | flops | bytes accessed | tf_op | source)
XLA Modules:
  0.0 233.5 jit_solution(5206758231770751808)
XLA Ops:
  7.2 0.9 broadcast_multiply_fusion.1
  8.5 0.2 select_reduce_fusion
  8.8 0.1 mul.146
  8.9 1.1 fusion.47
  10.0 1.1 fusion.49
  11.1 3.9 %scatter_custom_fusion = bf16[128,4096]{1,0:T(8,128)(2,1)} fusion(s32[64]{0:T(128)S(1)} %fusion.71, bf16[32,4096]{1,0:T(8,128)(2,1)S(1)} %fusion.49, s32[1024]{0:T(1024)S(1)} %pad_clamp_fusion.1, bf16[]{:T(256)} %constant.160.clone.1), kind=kCustom, calls=%fused_computation.70 | custom fusion | bytes 1048578 | tf_op jit(solution)/shard_map/scatter | solution.py:159
  15.1 7.3 %all-to-all-start = ((bf16[8,16,4096]{2,1,0:T(8,128)(2,1)}), bf16[8,16,4096]{2,1,0:T(8,128)(2,1)}, u32[]{:S(2)}, u32[]{:S(2)}) async-start(bf16[8,16,4096]{2,1,0:T(8,128)(2,1)} %bitcast.144), calls=%async_computation | async-start | bytes 2097152 | tf_op jit(solution)/shard_map/all_to_all | solution.py:160
  22.4 0.1 copy.57
  22.6 0.1 divide_multiply_fusion
  22.7 0.8 copy.58
  23.6 1.0 copy.62
  24.5 0.1 copy.63
  24.7 0.7 copy.89
  25.3 1.6 copy.60
  26.9 0.8 convert_bitcast_fusion
  27.9 1.7 reduce_window_sum.33
  29.6 18.6 %all-to-all-done = bf16[8,16,4096]{2,1,0:T(8,128)(2,1)} async-done(((bf16[8,16,4096]{2,1,0:T(8,128)(2,1)}), bf16[8,16,4096]{2,1,0:T(8,128)(2,1)}, u32[]{:S(2)}, u32[]{:S(2)}) %all-to-all-start) | async-done | bytes 1048608 | tf_op jit(solution)/shard_map/all_to_all | solution.py:160
  48.3 8.9 %while.27 = (s32[]{:T(128)}, f32[2,128,128]{2,1,0:T(8,128)S(1)}, f32[2,2,64,128]{3,2,0,1:T(8,128)}, f32[2,2,64,128]{3,2,0,1:T(8,128)}, f32[2,2,64,128]{3,2,0,1:T...) while((s32[]{:T(128)}, f32[2,128,128]{2,1,0:T(8,128)S(1)}, ...), condition=%wide.region_2.3_spmd.clone, body=%wide.region_0.2_spmd.clone.sunk | while | flops 76787712 | bytes 1623164 | solution.py:64
  48.3 0.9 dynamic-slice_bitcast_fusion.2
  49.3 1.1 convolution_select_fusion.2
  50.4 0.2 fusion.91
  50.6 1.7 fusion.92
  52.3 0.4 convolution_add_fusion.4
  52.8 0.9 dynamic-slice_bitcast_fusion.2
  53.7 1.1 convolution_select_fusion.2
  54.8 0.2 fusion.91
  55.0 1.7 fusion.92
  56.8 0.4 convolution_add_fusion.4
  57.2 0.6 convert_element_type.74
  57.9 0.7 slice.42
  58.6 18.6 %all-gather = bf16[16,1,128]{2,1,0:T(2,128)(2,1)S(1)} all-gather(bf16[2,1,128]{2,1,0:T(2,128)(2,1)S(1)} %slice.42), channel_id=2, replica_groups=mesh['ep'=8,'tp'=4] {'ep'}, dimensions={0}, use_global_device_ids=true | all-gather | bytes 4608 | tf_op jit(solution)/shard_map/all_gather | solution.py:17
  77.1 1.7 copy.71
  78.8 1.6 copy.72
  80.4 31.8 %all-gather.1 = bf16[16,128,128]{2,1,0:T(8,128)(2,1)S(1)} all-gather(bf16[2,128,128]{2,1,0:T(8,128)(2,1)} %convert_element_type.74), channel_id=3, replica_groups=mesh['ep'=8,'tp'=4] {'ep'}, dimensions={0}, use_global_device_ids=true | all-gather | bytes 589824 | tf_op jit(solution)/shard_map/all_gather | solution.py:17
  112.2 1.4 while.28
  112.2 0.1 fusion.93
  112.3 0.1 fusion.93
  112.5 0.1 fusion.93
  112.7 0.1 fusion.93
  112.9 0.1 fusion.93
  113.0 0.1 fusion.93
  113.2 0.1 fusion.93
  113.4 0.1 fusion.93
  113.5 1.4 multiply_reduce_fusion.1
  115.0 0.9 fusion.58
  116.0 2.8 %fusion.32 = bf16[640,4096]{1,0:T(8,128)(2,1)} fusion(bf16[256,4096]{1,0:T(8,128)(2,1)} %param.26, bf16[128,256]{0,1:T(8,128)(2,1)S(1)} %fusion.58), kind=kOutput, calls=%fused_computation.52 | convolution fusion | flops 67239936 | bytes 2424832 | tf_op jit(solution)/shard_map/dot_general | solution.py:179
  118.8 4.9 %fusion.39 = f32[512,352]{0,1:T(8,128)S(1)} fusion(bf16[512,4096]{1,0:T(8,128)(2,1)} %bitcast.156, bf16[1,4096,352]{1,2,0:T(8,128)(2,1)} %param.31), kind=kOutput, calls=%fused_computation.59 | convolution fusion | flops 1476395008 | bytes 7798784 | tf_op jit(solution)/shard_map/dot_general | solution.py:89
  123.7 0.2 copy-done.9
  123.9 1.7 fusion.44
  125.7 1.7 fusion.28
  127.4 1.3 fusion.31
  128.7 1.7 fusion.27
  130.4 1.3 fusion.30
  131.7 1.7 fusion.26
  133.4 1.3 fusion.29
  134.7 1.7 fusion.25
  136.4 48.8 %reduce-scatter.2.cloned.1.call-done = bf16[160,4096]{1,0:T(8,128)(2,1)} async-done(((bf16[640,4096]{1,0:T(8,128)(2,1)}), bf16[160,4096]{1,0:T(8,128)(2,1)}) %reduce-scatter.2.cloned.1.call-update) | async-done | bytes 1310736 | tf_op jit(solution)/shard_map/reduce_scatter | solution.py:182
  185.2 2.4 %slice.38 = bf16[128,4096]{1,0:T(8,128)(2,1)} slice(bf16[160,4096]{1,0:T(8,128)(2,1)} %reduce-scatter.2.cloned.1.call-done), slice={[32:160], [0:4096]} | slice | bytes 2097152 | tf_op jit(solution)/shard_map/slice | solution.py:186
  187.6 5.5 %all-to-all-start.1 = ((bf16[8,16,4096]{2,1,0:T(8,128)(2,1)}), bf16[8,16,4096]{2,1,0:T(8,128)(2,1)}, u32[]{:S(2)}, u32[]{:S(2)}) async-start(bf16[8,16,4096]{2,1,0:T(8,128)(2,1)} %bitcast.145), calls=%async_computation.2 | async-start | bytes 2097152 | tf_op jit(solution)/shard_map/all_to_all | solution.py:187
  193.3 1.7 slice.37
  195.0 23.9 %all-to-all-done.1 = bf16[8,16,4096]{2,1,0:T(8,128)(2,1)} async-done(((bf16[8,16,4096]{2,1,0:T(8,128)(2,1)}), bf16[8,16,4096]{2,1,0:T(8,128)(2,1)}, u32[]{:S(2)}, u32[]{:S(2)}) %all-to-all-start.1) | async-done | bytes 1048608 | tf_op jit(solution)/shard_map/all_to_all | solution.py:187
  218.9 2.7 %gather_fusion = bf16[64,4096]{1,0:T(8,128)(2,1)S(1)} fusion(bf16[128,4096]{1,0:T(8,128)(2,1)} %bitcast.30, s32[1024]{0:T(1024)S(1)} %pad_clamp_fusion), kind=kCustom, calls=%fused_computation.1 | custom fusion | bytes 1048832 | tf_op jit(solution)/shard_map/gather | solution.py:194
  221.6 1.6 reshape.200
  223.2 3.4 %multiply_reduce_fusion = bf16[32,4096]{1,0:T(8,128)(2,1)} fusion(f32[32,2,4096]{2,1,0:T(2,128)} %reshape.200, f32[32,2]{1,0:T(8,128)S(1)} %copy.75), kind=kLoop, calls=%fused_computation.64 | loop fusion | flops 393216 | bytes 1310976 | tf_op jit(solution)/shard_map/reduce_sum | solution.py:196
  (63 shorter events, 1.3 us)
Async XLA Ops:
  7.2 118.5 %copy-start = (bf16[1,352,4096]{2,1,0:T(8,128)(2,1)S(1)}, bf16[1,352,4096]{2,1,0:T(8,128)(2,1)}, u32[]{:S(2)}) copy-start(bf16[1,352,4096]{2,1,0:T(8,128)(2,1)} %param.33) | copy-start | bytes 8650756
  7.2 15.2 %copy-start.3 = (bf16[128,256]{1,0:T(8,128)(2,1)S(1)}, bf16[128,256]{1,0:T(8,128)(2,1)}, u32[]{:S(2)}) copy-start(bf16[128,256]{1,0:T(8,128)(2,1)} %param.20) | copy-start | bytes 196612
  7.2 15.4 %copy-start.5 = (f32[256]{0:T(256)S(1)}, f32[256]{0:T(256)}, u32[]{:S(2)}) copy-start(f32[256]{0:T(256)} %param.23) | copy-start | bytes 3076
  7.2 15.5 %copy-start.6 = (f32[2,128]{1,0:T(2,128)S(1)}, f32[2,128]{1,0:T(2,128)}, u32[]{:S(2)}) copy-start(f32[2,128]{1,0:T(2,128)} %param.24) | copy-start | bytes 3076
  15.1 33.2 %all-to-all-start = ((bf16[8,16,4096]{2,1,0:T(8,128)(2,1)}), bf16[8,16,4096]{2,1,0:T(8,128)(2,1)}, u32[]{:S(2)}, u32[]{:S(2)}) async-start(bf16[8,16,4096]{2,1,0:T(8,128)(2,1)} %bitcast.144), calls=%async_computation | async-start | bytes 2097152 | tf_op jit(solution)/shard_map/all_to_all | solution.py:160
  22.4 96.4 %all-gather.4.cloned.1.call-start = ((), (), s32[]{:S(2)}) async-start(), calls=%async_computation.3 | async-start | bytes 5242880 | tf_op jit(solution)/shard_map/all_gather | solution.py:163
  24.7 2.3 copy-start.2
  48.2 137.0 %reduce-scatter.2.cloned.1.call-start = ((), (), s32[]{:S(2)}) async-start(), calls=%async_computation.4 | async-start | bytes 6553600 | tf_op jit(solution)/shard_map/reduce_scatter | solution.py:182
  57.2 57.8 %copy-start.7 = (f32[256]{0:T(256)S(1)}, f32[256]{0:T(256)}, u32[]{:S(2)}) copy-start(f32[256]{0:T(256)} %param.25) | copy-start | bytes 3076
  118.7 4.9 %copy-start.8 = (bf16[32,16,4096]{2,1,0:T(8,128)(2,1)S(1)}, bf16[32,16,4096]{2,1,0:T(8,128)(2,1)}, u32[]{:S(2)}) copy-start(bf16[32,16,4096]{2,1,0:T(8,128)(2,1)} %all-gather.4.cloned.1.call-done) | copy-start | bytes 12582916
  118.7 5.2 %copy-start.9 = (bf16[1,4096,352]{1,2,0:T(8,128)(2,1)S(1)}, bf16[1,4096,352]{1,2,0:T(8,128)(2,1)}, u32[]{:S(2)}) copy-start(bf16[1,4096,352]{1,2,0:T(8,128)(2,1)} %param.32) | copy-start | bytes 8650756
  125.7 1.7 copy-start.1
  136.4 56.7 %copy-start.4 = (f32[32,2]{0,1:T(2,128)S(1)}, f32[32,2]{0,1:T(2,128)}, u32[]{:S(2)}) copy-start(f32[32,2]{0,1:T(2,128)} %param.30) | copy-start | bytes 772
  187.6 31.3 %all-to-all-start.1 = ((bf16[8,16,4096]{2,1,0:T(8,128)(2,1)}), bf16[8,16,4096]{2,1,0:T(8,128)(2,1)}, u32[]{:S(2)}, u32[]{:S(2)}) async-start(bf16[8,16,4096]{2,1,0:T(8,128)(2,1)} %bitcast.145), calls=%async_computation.2 | async-start | bytes 2097152 | tf_op jit(solution)/shard_map/all_to_all | solution.py:187
Sparse Core Ops, SparseCore 0:
  48.4 33.4 all-gather.3
  136.6 48.6 reduce-scatter.1
where the time goes:
time: 235 us; the launch traced here: 233 us
  waiting for transfers between devices  91.4 us (39%)
  blocking collectives  50.3 us (21%)
  matrix products  28.5 us (12%)
  local copies, waits for them, and re-layouts  23.1 us (10%)
  between operations  14.4 us (6%)
  starting transfers between devices  12.9 us (5%)
  other arithmetic  12.6 us (5%)
    all_gather x2, blocking collectives, entering_2(): lax.all_gather(part.astype(kind), axis)  50.3 us
    reduce_scatter x1, waiting for transfers between devices, per_device(): lax.psum_scatter(jnp.concatenate(pieces, axis=0).astype(jnp.bfloat16), 't...  48.8 us
    all_to_all x1, waiting for transfers between devices, per_device(): lax.all_to_all(expert_rows.reshape(expert_count, capacity, width), 'ep',...  23.9 us
    all_to_all x1, waiting for transfers between devices, per_device(): lax.all_to_all(buffer.reshape(expert_count, capacity, width), 'ep', split...  18.6 us
    all_to_all x1, starting transfers between devices, per_device(): lax.all_to_all(buffer.reshape(expert_count, capacity, width), 'ep', split...  7.28 us
    dot_general x4, matrix products, per_device(): jnp.dot(expert_part, down_local, preferred_element_type=jnp.float32)  6.89 us
    dot_general x4, matrix products, per_device(): jnp.dot(mix_part, recurrence_output_matrix, preferred_element_type=jnp.fl...  6.63 us
    all_to_all x1, starting transfers between devices, per_device(): lax.all_to_all(expert_rows.reshape(expert_count, capacity, width), 'ep',...  5.53 us
  transfers between devices with their start and end apart: 4, of which 3 were waited for; matrix products, arithmetic and copies ran while one was open for 12% of the time, Pallas kernels for 0%

commit v1 on v0

v1 whole, which is shorter than its diff:
```python
import functools

import jax
import jax.numpy as jnp
from jax import lax
from jax.experimental import pallas as pl
from jax.experimental.pallas import tpu as pltpu
from jax.sharding import PartitionSpec as P

TOP = 2
SPAN = 64
MESH = pl.DeviceIdType.MESH


epsilon = 1e-06
highest = lax.Precision.HIGHEST


def visiting_order(count):
    return sorted(range(1, count), key=lambda k: abs(k - count // 2)) + [0]


def greet(me, tp, ep_count, tp_count):
    pairs = tp_count // 2
    pair, side = tp // 2, tp % 2
    barrier = pltpu.get_barrier_semaphore()
    for k in range(1, ep_count):
        pl.semaphore_signal(
            barrier,
            inc=1,
            device_id={"ep": lax.rem(me + k, ep_count), "tp": tp},
            device_id_type=MESH,
        )
    for j in range(1, pairs):
        pl.semaphore_signal(
            barrier,
            inc=1,
            device_id={"ep": me, "tp": lax.rem(pair + j, pairs) * 2 + side},
            device_id_type=MESH,
        )
    pl.semaphore_signal(
        barrier, inc=1, device_id={"ep": me, "tp": pair * 2 + 1 - side}, device_id_type=MESH
    )
    pl.semaphore_wait(barrier, ep_count + pairs - 1)


def dispatch_kernel(
    ep_count, tp_count, slots, state, piece, states, sa, ra, sy, ry, sc, rc, ss, rs
):
    me, tp = lax.axis_index("ep"), lax.axis_index("tp")
    pairs = tp_count // 2
    pair, side = tp // 2, tp % 2
    other = pair * 2 + 1 - side
    order = visiting_order(ep_count)

    def remote(src, dst, send, recv, ep, to):
        return pltpu.make_async_remote_copy(
            src_ref=src,
            dst_ref=dst,
            send_sem=send,
            recv_sem=recv,
            device_id={"ep": ep, "tp": to},
            device_id_type=MESH,
        )

    states[...] = jnp.zeros_like(states)
    greet(me, tp, ep_count, tp_count)

    def exchange(k):
        to = lax.rem(me + k, ep_count)
        return remote(slots.at[to], piece.at[tp, me], sa.at[k], ra.at[k], to, tp)

    def state_copy(k):
        to = lax.rem(me + k, ep_count)
        return remote(state, states.at[me], ss.at[k], rs.at[k], to, tp)

    for k in order[:-1]:
        exchange(k).start()

    def source(k):
        return lax.rem(me + ep_count - k, ep_count)

    def own_block(k):
        return slots.at[me] if k == 0 else piece.at[tp, source(k)]

    def across(k, j):
        to = lax.rem(pair + j, pairs) * 2 + side
        return remote(own_block(k), piece.at[tp, source(k)], sy.at[j, k], ry.at[j, k], me, to)

    def beside(k, j):
        block = lax.rem(pair + pairs - j, pairs) * 2 + side
        src = own_block(k) if j == 0 else piece.at[block, source(k)]
        return remote(src, piece.at[block, source(k)], sc.at[j, k], rc.at[j, k], me, other)

    def pass_on(k):
        for j in range(1, pairs):
            across(k, j).start()
        beside(k, 0).start()

    pass_on(0)
    for k in range(1, ep_count):

        @pl.when(me + k < ep_count)
        def _(k=k):
            state_copy(k).start()

    piece[tp, me] = slots[me]
    sequence = [0] + order[:-1]
    for position, k in enumerate(sequence):
        if k:
            exchange(k).wait_recv()
            pass_on(k)
        if position:
            before = sequence[position - 1]
            for j in range(1, pairs):
                across(before, j).wait_recv()
                beside(before, j).start()
    for j in range(1, pairs):
        across(sequence[-1], j).wait_recv()
        beside(sequence[-1], j).start()
    for k in range(1, ep_count):

        @pl.when(me + k < ep_count)
        def _(k=k):
            state_copy(k).wait_send()

        @pl.when(me - k >= 0)
        def _(k=k):
            state_copy(k).wait_recv()

        exchange(k).wait_send()
    for k in sequence:
        for j in range(pairs):
            if j:
                across(k, j).wait_send()
            beside(k, j).wait_send()
            beside(k, j).wait_recv()


def dispatch(slots, state, ep_count, tp_count):
    pairs = tp_count // 2
    dma = pltpu.SemaphoreType.DMA
    vmem = pl.BlockSpec(memory_space=pltpu.VMEM)
    return pl.pallas_call(
        functools.partial(dispatch_kernel, ep_count, tp_count),
        out_shape=(
            jax.ShapeDtypeStruct((tp_count,) + slots.shape, slots.dtype),
            jax.ShapeDtypeStruct((ep_count,) + state.shape, state.dtype),
        ),
        in_specs=[vmem] * 2,
        out_specs=(vmem, vmem),
        scratch_shapes=[
            dma((ep_count,)),
            dma((ep_count,)),
            dma((pairs, ep_count)),
            dma((pairs, ep_count)),
            dma((pairs, ep_count)),
            dma((pairs, ep_count)),
            dma((ep_count,)),
            dma((ep_count,)),
        ],
        compiler_params=pltpu.CompilerParams(collective_id=0, has_side_effects=True),
    )(slots, state)


def return_kernel(
    ep_count,
    tp_count,
    parts,
    mix,
    mixed,
    returned,
    cbuf,
    cmix,
    ysend,
    ysmix,
    ybuf,
    ymix,
    abuf,
    sc,
    rc,
    sy,
    ry,
    sa,
    ra,
):
    me, tp = lax.axis_index("ep"), lax.axis_index("tp")
    pairs = tp_count // 2
    pair, side = tp // 2, tp % 2
    other = pair * 2 + 1 - side
    order = visiting_order(ep_count)
    greet(me, tp, ep_count, tp_count)

    def remote(src, dst, send, recv, ep, to):
        return pltpu.make_async_remote_copy(
            src_ref=src,
            dst_ref=dst,
            send_sem=send,
            recv_sem=recv,
            device_id={"ep": ep, "tp": to},
            device_id_type=MESH,
        )

    def chunk(k):
        return lax.rem(me + k, ep_count)

    def toward(j):
        return lax.rem(pair + j, pairs)

    def beside(k, j):
        block = toward(j) * 2 + 1 - side
        if k == ep_count:
            return remote(mix.at[block], cmix.at[j], sc.at[j, k], rc.at[j, k], me, other)
        return remote(parts.at[block, chunk(k)], cbuf.at[j, k], sc.at[j, k], rc.at[j, k], me, other)

    def across(k, j):
        to = toward(j) * 2 + side
        if k == ep_count:
            return remote(ysmix.at[j], ymix.at[j], sy.at[j, k], ry.at[j, k], me, to)
        return remote(ysend.at[j, k], ybuf.at[j, k], sy.at[j, k], ry.at[j, k], me, to)

    def home(k):
        return remote(abuf.at[k], returned.at[me], sa.at[k], ra.at[k], chunk(k), tp)

    wide = jnp.float32
    everything = order + [ep_count]
    for k in everything:
        for j in list(range(1, pairs)) + [0]:
            beside(k, j).start()
    for k in everything:
        for j in range(1, pairs):
            beside(k, j).wait_recv()
            block = toward(j) * 2 + side
            if k == ep_count:
                ysmix[j] = (mix[block].astype(wide) + cmix[j].astype(wide)).astype(mix.dtype)
            else:
                ysend[j, k] = (
                    parts[block, chunk(k)].astype(wide) + cbuf[j, k].astype(wide)
                ).astype(parts.dtype)
            across(k, j).start()
    for k in everything:
        beside(k, 0).wait_recv()
        if k == ep_count:
            total = mix[tp].astype(wide) + cmix[0].astype(wide)
        else:
            total = parts[tp, chunk(k)].astype(wide) + cbuf[0, k].astype(wide)
        for j in range(1, pairs):
            across(k, j).wait_recv()
            total = total + (ymix[j] if k == ep_count else ybuf[j, k]).astype(wide)
        total = total.astype(parts.dtype)
        if k == ep_count:
            mixed[...] = total
        elif k == 0:
            returned[me] = total
        else:
            abuf[k] = total
            home(k).start()
    for k in everything:
        for j in range(pairs):
            beside(k, j).wait_send()
            if j:
                across(k, j).wait_send()
        if 0 < k < ep_count:
            home(k).wait()


def give_back(parts, mix, ep_count, tp_count):
    pairs = tp_count // 2
    dma = pltpu.SemaphoreType.DMA
    vmem = pl.BlockSpec(memory_space=pltpu.VMEM)
    chunks, rows = parts.shape[1:], mix.shape[1:]
    many = (pairs, ep_count + 1)
    kind = parts.dtype
    return pl.pallas_call(
        functools.partial(return_kernel, ep_count, tp_count),
        out_shape=(
            jax.ShapeDtypeStruct(rows, kind),
            jax.ShapeDtypeStruct(chunks, kind),
        ),
        in_specs=[vmem] * 2,
        out_specs=(vmem, vmem),
        scratch_shapes=[
            pltpu.VMEM((pairs,) + chunks, kind),
            pltpu.VMEM((pairs,) + rows, kind),
            pltpu.VMEM((pairs,) + chunks, kind),
            pltpu.VMEM((pairs,) + rows, kind),
            pltpu.VMEM((pairs,) + chunks, kind),
            pltpu.VMEM((pairs,) + rows, kind),
            pltpu.VMEM(chunks, kind),
            dma(many),
            dma(many),
            dma(many),
            dma(many),
            dma((ep_count,)),
            dma((ep_count,)),
        ],
        compiler_params=pltpu.CompilerParams(collective_id=1, has_side_effects=True),
    )(parts, mix)


def span_recurrence(query, inflow, decay_logarithm, values):
    number_of_heads, seq_len, key_width = query.shape
    span_count = seq_len // SPAN

    def to_spans(array):
        return array.reshape(number_of_heads, span_count, SPAN, array.shape[-1]).transpose(
            1, 0, 2, 3
        )

    lower_mask = jnp.tril(jnp.ones((SPAN, SPAN), bool))

    def advance(carried, inputs):
        query_span, inflow_span, decay_span, value_span = inputs
        running = jnp.cumsum(decay_span, axis=1)
        lifted_query = query_span * jnp.exp(running)
        lowered_inflow = inflow_span * jnp.exp(-running)
        scores = jnp.einsum("htd,hsd->hts", lifted_query, lowered_inflow, precision=highest)
        scores = jnp.where(lower_mask[None, :, :], scores, 0.0)
        output = jnp.einsum("hts,hsv->htv", scores, value_span, precision=highest)
        output = output + jnp.einsum("htd,hdv->htv", lifted_query, carried, precision=highest)
        closing = running[:, -1:, :]
        updated = jnp.exp(closing[:, 0, :])[:, :, None] * carried + jnp.einsum(
            "hsd,hsv->hdv", inflow_span * jnp.exp(closing - running), value_span, precision=highest
        )
        return (updated, output)

    start_state = jnp.zeros((number_of_heads, key_width, values.shape[-1]), jnp.float32)
    final_state, outputs = lax.scan(
        advance,
        start_state,
        (to_spans(query), to_spans(inflow), to_spans(decay_logarithm), to_spans(values)),
        unroll=True,
    )
    return (
        final_state,
        outputs.transpose(1, 0, 2, 3).reshape(number_of_heads, seq_len, values.shape[-1]),
    )


def slot_positions(block_routes, expert_count):
    chosen = block_routes.reshape(-1)
    table = (chosen[:, None] == jnp.arange(expert_count, dtype=jnp.int32)[None, :]).astype(
        jnp.int32
    )
    before = jnp.cumsum(table, axis=0) - table
    return (chosen, jnp.sum(before * table, axis=1))


def expert_hidden(flat_rows, gate_local, up_local):
    gate_proj = jnp.dot(flat_rows, gate_local, preferred_element_type=jnp.float32)
    up_proj = jnp.dot(flat_rows, up_local, preferred_element_type=jnp.float32)
    return (jax.nn.silu(gate_proj) * up_proj).astype(jnp.bfloat16)


def per_device(
    recurrence_query,
    forget_preactivation,
    recurrence_value,
    output_gate_preactivation,
    forget_margin,
    surge_log_decay,
    head_norm_gain,
    recurrence_output_matrix,
    second_micro_input,
    expert_norm_gain,
    routes,
    router_chosen_logits,
    expert_gate_matrix,
    expert_up_matrix,
    expert_down_matrix,
):
    number_of_heads = surge_log_decay.shape[0]
    seq_len = recurrence_query.shape[0]

    def heads_leading(array):
        return array.astype(jnp.float32).reshape(seq_len, number_of_heads, -1).transpose(1, 0, 2)

    closed_flag = jax.nn.sigmoid(-forget_preactivation.astype(jnp.float32)) * forget_margin
    decay_logarithm = heads_leading(jnp.log1p(-closed_flag)) + surge_log_decay[:, :, None]
    query = heads_leading(recurrence_query)
    final_state, local_out = span_recurrence(
        query, heads_leading(closed_flag), decay_logarithm, heads_leading(recurrence_value)
    )
    running = jnp.cumsum(decay_logarithm, axis=1)
    totals = running[:, -1, :]
    tp_count = lax.axis_size("tp")
    tp_rank = lax.axis_index("tp")
    ep_rank = lax.axis_index("ep")
    expert_count = lax.axis_size("ep")
    tok_rows = second_micro_input.shape[0]
    width = second_micro_input.shape[1]
    capacity = 2 * tok_rows * TOP // expert_count
    moe_rows = second_micro_input.astype(jnp.float32)
    normed = (
        moe_rows
        * lax.rsqrt(jnp.mean(moe_rows * moe_rows, axis=-1, keepdims=True) + epsilon)
        * expert_norm_gain
    ).astype(jnp.bfloat16)
    own_routes = lax.dynamic_slice_in_dim(routes, tp_rank * tok_rows, tok_rows, 0)
    own_chosen, own_places = slot_positions(own_routes, expert_count)
    spot = (own_chosen * capacity + own_places).reshape(tok_rows, TOP)
    numbers = jnp.arange(expert_count * capacity, dtype=jnp.int32)
    taken = spot[:, :, None] == numbers
    chooser = jnp.sum(taken.astype(jnp.bfloat16), axis=1)
    slots = jnp.dot(chooser.T, normed, preferred_element_type=jnp.float32).astype(jnp.bfloat16)
    slots = slots.reshape(expert_count, capacity, width)
    coarse = totals.astype(jnp.bfloat16)
    fine = (totals - coarse.astype(jnp.float32)).astype(jnp.bfloat16)
    packed = jnp.concatenate(
        [
            final_state.astype(jnp.bfloat16),
            jnp.swapaxes(jnp.stack([coarse, fine], axis=-1), 1, 2),
        ],
        axis=1,
    )
    piece, states = dispatch(slots, packed, expert_count, tp_count)
    key_rows = final_state.shape[1]
    ranks = jnp.arange(expert_count)
    all_totals = jnp.sum(states[:, :, key_rows:, :].astype(jnp.float32), axis=2)
    between = (ranks[None, :] > ranks[:, None]) & (ranks[None, :] < ep_rank)
    spans_after = jnp.sum(jnp.where(between[:, :, None, None], all_totals[None], 0.0), axis=1)
    survive = jnp.where((ranks < ep_rank)[:, None, None], jnp.exp(spans_after), 0.0)
    entering = jnp.sum(
        survive[:, :, :, None] * states[:, :, :key_rows, :].astype(jnp.float32), axis=0
    )
    output = local_out + jnp.einsum(
        "htd,hdv->htv", query * jnp.exp(running), entering, precision=highest
    )
    output = output * lax.rsqrt(jnp.mean(output * output, axis=-1, keepdims=True) + epsilon)
    output = output.transpose(1, 0, 2).reshape(seq_len, -1)
    hidden_a = (
        output * head_norm_gain * jax.nn.silu(output_gate_preactivation.astype(jnp.float32))
    ).astype(jnp.bfloat16)
    hidden_b = expert_hidden(
        piece.reshape(-1, width), expert_gate_matrix[0], expert_up_matrix[0]
    )
    mix_rows = seq_len // tp_count
    mix_parts = jnp.dot(
        hidden_a, recurrence_output_matrix, preferred_element_type=jnp.float32
    ).astype(jnp.bfloat16)
    expert_parts = jnp.dot(
        hidden_b, expert_down_matrix[0], preferred_element_type=jnp.float32
    ).astype(jnp.bfloat16)
    mixed, returned = give_back(
        expert_parts.reshape(piece.shape),
        mix_parts.reshape(tp_count, mix_rows, width),
        expert_count,
        tp_count,
    )
    route_weight = jax.nn.softmax(router_chosen_logits, axis=-1)
    weights = jnp.sum(jnp.where(taken, route_weight[:, :, None], 0.0), axis=1)
    moe_out = jnp.dot(
        weights, returned.reshape(-1, width).astype(jnp.float32), precision=highest
    )
    return (mixed, moe_out.astype(jnp.bfloat16))


def solution(mesh):
    return jax.shard_map(
        per_device,
        mesh=mesh,
        in_specs=(
            P("ep", "tp"),
            P("ep", "tp"),
            P("ep", "tp"),
            P("ep", "tp"),
            P("tp"),
            P("tp", "ep"),
            P("tp"),
            P("tp", None),
            P(("ep", "tp"), None),
            P(),
            P("ep", None),
            P(("ep", "tp"), None),
            P("ep", None, "tp"),
            P("ep", None, "tp"),
            P("ep", "tp", None),
        ),
        out_specs=(P(("ep", "tp"), None), P(("ep", "tp"), None)),
        check_vma=False,
    )
```

time: 235 us -> 147 us (0.63)
  Pallas kernels: 0 us -> 91.6 us
  waiting for transfers between devices: 91.4 us -> 0 us
  blocking collectives: 50.3 us -> 0 us
  between operations: 14.4 us -> 0.95 us
  starting transfers between devices: 12.9 us -> 0 us
  local copies, waits for them, and re-layouts: 23.1 us -> 11.7 us
  other arithmetic: 12.6 us -> 15.8 us
    pallas_call x0 -> x2, Pallas kernels: none -> 91.6 us  [the longest x1 48.3 us: dispatch(): pl.pallas_call(functools.partial(dispatch_kernel, ep_count, tp_count), ou...]
    all_gather x2 -> x0, blocking collectives: 50.3 us -> none  [entering_2(): lax.all_gather(part.astype(kind), axis)]
    reduce_scatter x1 -> x0, waiting for transfers between devices: 48.8 us -> none  [per_device(): lax.psum_scatter(jnp.concatenate(pieces, axis=0).astype(jnp.bfloat16), 't...]
    all_to_all x2 -> x0, waiting for transfers between devices: 42.6 us -> none  [the longest x1 23.9 us: per_device(): lax.all_to_all(expert_rows.reshape(expert_count, capacity, width), 'ep',...]
    all_to_all x2 -> x0, starting transfers between devices: 12.8 us -> none  [the longest x1 7.28 us: per_device(): lax.all_to_all(buffer.reshape(expert_count, capacity, width), 'ep', split...]
    slice x3 -> x0, local copies, waits for them, and re-layouts: 4.72 us -> none  [the longest x1 2.35 us: per_device(): expert_rows = summed[mix_rows:].astype(jnp.bfloat16)]
    scatter x1 -> x0, local copies, waits for them, and re-layouts: 3.94 us -> none  [per_device(): buffer.at[own_chosen * capacity + own_places].set(normed[copy_source])]
    dot_general x2, matrix products: 3.48 us -> 0.45 us  [advance(): jnp.einsum('htd,hdv->htv', lifted_query, carried, precision=highest)]
  transfers between devices with their start and end apart: 4 -> 0, of which waited for: 3 -> 0; matrix products, arithmetic and copies ran while one was open for 12% -> 0% of each run, Pallas kernels for 0% -> 0%
where the time goes in v1:
time: 147 us; the launch traced here: 146 us
  Pallas kernels  91.6 us (62%)
  matrix products  26.4 us (18%)
  other arithmetic  15.8 us (11%)
  local copies, waits for them, and re-layouts  11.7 us (8%)
    pallas_call x1, Pallas kernels, dispatch(): pl.pallas_call(functools.partial(dispatch_kernel, ep_count, tp_count), ou...  48.3 us
    pallas_call x1, Pallas kernels, give_back(): pl.pallas_call(functools.partial(return_kernel, ep_count, tp_count), out_...  43.2 us
    dot_general x1, matrix products, per_device(): jnp.dot(hidden_b, expert_down_matrix[0], preferred_element_type=jnp.float32)  9.17 us
    unnamed x18, local copies, waits for them, and re-layouts  6.21 us
    dot_general x1, matrix products, expert_hidden(): jnp.dot(flat_rows, gate_local, preferred_element_type=jnp.float32)  5.7 us
    dot_general x1, matrix products, per_device(): jnp.dot(hidden_a, recurrence_output_matrix, preferred_element_type=jnp.fl...  3.1 us

profile of v1, /device:TPU:0, one launch (start us, length us, event | category | flops | bytes accessed | tf_op | source)
XLA Modules:
  0.0 146.4 jit_solution(8211589498846551541)
XLA Ops:
  0.6 0.0 copy-start
  0.7 0.0 copy-start.5
  0.7 0.8 reduce_max.9
  1.5 0.7 fusion.57
  2.2 0.7 fusion.56
  2.9 0.8 constant_dynamic-slice_fusion
  3.7 1.1 fusion.16
  4.8 0.6 add_rsqrt_fusion.1
  5.3 0.6 fusion.55
  5.9 0.0 copy-done.5
  5.9 0.1 copy.109
  6.0 0.1 eq.28
  6.1 0.1 fusion.51
  6.2 0.1 reduce_window_sum.39
  6.3 0.2 select_reduce_fusion.2
  6.5 0.1 reduce_sum.87
  6.6 0.1 copy.90
  6.7 0.1 fusion.54
  6.8 0.7 select_reduce_fusion.1
  7.5 0.9 copy.100
  8.4 0.1 copy.101
  8.5 1.0 copy.91
  9.5 1.0 copy.96
  10.5 0.1 copy.97
  10.6 1.6 %copy.107 = bf16[128,256]{0,1:T(8,128)(2,1)} copy(bf16[128,256]{1,0:T(8,128)(2,1)} %param.18) | data formatting | bytes 131072 | tf_op args[3]
  12.2 1.4 divide_multiply_fusion
  13.6 1.7 %copy.94 = f32[2,128,128]{2,1,0:T(8,128)} copy(f32[2,128,128]{1,2,0:T(8,128)} %bitcast.142) | data formatting | bytes 262144 | tf_op jit(solution)/shard_map/transpose | solution.py:376
  15.3 0.8 copy.92
  16.1 1.0 bitcast_add_fusion
  17.1 0.8 reduce_window_sum.42
  17.9 0.7 subtract_convert_fusion
  18.6 0.7 fusion.58
  19.3 0.6 maximum_bitcast_fusion.1
  19.9 0.1 reduce_window_sum.40
  20.0 0.1 reduce_window_sum.41
  20.2 0.9 copy_bitcast_fusion
  21.1 0.2 convolution_select_fusion
  21.4 0.2 fusion.53
  21.5 0.2 convolution_select_fusion.1
  21.8 0.2 fusion.52
  21.9 0.2 fusion.13
  22.1 0.3 convolution_add_fusion.2
  22.4 0.0 copy-start.4
  22.5 0.9 fusion.11
  23.4 0.3 fusion.12
  23.7 0.1 copy.106
  23.8 0.0 copy-start.2
  23.8 1.5 %pad_maximum_fusion.state = bf16[2,130,128]{2,1,0:T(8,128)(2,1)} fusion(bf16[2,2,128]{2,1,0:T(2,128)(2,1)} %maximum_bitcast_fusion.1, bf16[2,128,128]{2,1,0:T(8,128)(2,1)} %fusion.11), kind=kLoop, calls=%fused_computation.48 | loop fusion | flops 133120 | bytes 133120 | tf_op jit(solution)/shard_map/concatenate | solution.py:409
  25.3 0.0 copy-done.1
  25.3 2.2 %convolution_convert_fusion.2 = bf16[128,4096]{1,0:T(8,128)(2,1)} fusion(bf16[32,128]{1,0:T(8,128)(2,1)S(1)} %fusion.54, bf16[32,4096]{1,0:T(8,128)(2,1)S(1)} %copy-done.1, f32[4096]{0:T(1024)} %param.24, f32[32]{0:T(128)} %add_rsqrt_fusion.1), kind=kOutput, calls=%fused_computation.2 | convolution fusion | flops 34603008 | bytes 1335424 | tf_op jit(solution)/shard_map/dot_general | solution.py:405
  27.5 48.3 %shard_map.158 = (bf16[4,8,16,4096]{3,2,1,0:T(8,128)(2,1)}, bf16[8,2,130,128]{3,2,1,0:T(8,128)(2,1)}) custom-call(bf16[8,16,4096]{2,1,0:T(8,128)(2,1)} %bitcast.133, bf16[2,130,128]{2,1,0:T(8,128)(2,1)} %pad_maximum_fusion.state), custom_call_target="tpu_custom_call" | custom-call | tf_op jit(solution)/shard_map/pallas_call | solution.py:144
  75.8 0.8 convert_reduce_fusion
  76.6 0.8 select_reduce_fusion
  77.4 0.8 exponential_select_fusion
  78.2 1.4 multiply_reduce_fusion
  79.5 1.3 multiply_reduce_fusion.1
  80.9 0.0 copy-done.4
  80.9 0.1 fusion.28
  81.0 5.7 %fusion.3 = f32[512,352]{0,1:T(8,128)} fusion(bf16[512,4096]{1,0:T(8,128)(2,1)} %bitcast.153, bf16[1,4096,352]{1,2,0:T(8,128)(2,1)} %param.27), kind=kOutput, calls=%fused_computation.7 | convolution fusion | flops 1476395008 | bytes 7798784 | tf_op jit(solution)/shard_map/dot_general | solution.py:350
  86.7 9.2 %convolution_convert_fusion = bf16[512,4096]{1,0:T(8,128)(2,1)} fusion(bf16[1,352,4096]{2,1,0:T(8,128)(2,1)S(1)} %copy-done, bf16[512,4096]{1,0:T(8,128)(2,1)} %bitcast.154, bf16[1,4096,352]{1,2,0:T(8,128)(2,1)} %param.28, f32[512,352]{0,1:T(8,128)} %fusion.3), kind=kOutput, calls=%fused_computation | convolution fusion | flops 2955968512 | bytes 14876672 | tf_op jit(solution)/shard_map/dot_general | solution.py:441
  95.9 3.1 %convolution_convert_fusion.1 = bf16[128,4096]{1,0:T(8,128)(2,1)} fusion(bf16[128,256]{0,1:T(8,128)(2,1)S(1)} %fusion.28, bf16[256,4096]{1,0:T(8,128)(2,1)} %param.22), kind=kOutput, calls=%fused_computation.1 | convolution fusion | flops 268959744 | bytes 3211264 | tf_op jit(solution)/shard_map/dot_general | solution.py:438
  99.0 43.2 %shard_map.159 = (bf16[32,4096]{1,0:T(8,128)(2,1)}, bf16[8,16,4096]{2,1,0:T(8,128)(2,1)}) custom-call(bf16[4,8,16,4096]{3,2,1,0:T(8,128)(2,1)} %bitcast.132, bf16[4,32,4096]{2,1,0:T(8,128)(2,1)} %bitcast.131), custom_call_target="tpu_custom_call" | custom-call | tf_op jit(solution)/shard_map/pallas_call | solution.py:274
  142.2 2.5 %convolution_convert_fusion.3 = bf16[32,4096]{1,0:T(8,128)(2,1)} fusion(f32[32,128]{1,0:T(8,128)S(1)} %copy-done.3, bf16[128,4096]{1,0:T(8,128)(2,1)} %bitcast.136), kind=kOutput, calls=%fused_computation.3 | convolution fusion | flops 201457664 | bytes 1327104 | tf_op jit(solution)/shard_map/dot_general | solution.py:452
  144.7 1.7 %copy.118 = bf16[32,4096]{1,0:T(8,128)(2,1)} copy(bf16[32,4096]{1,0:T(8,128)(2,1)} %get-tuple-element.20) | data formatting | bytes 524288
  (20 shorter events, 0.1 us)
Async XLA Ops:
  0.6 86.1 %copy-start = (bf16[1,352,4096]{2,1,0:T(8,128)(2,1)S(1)}, bf16[1,352,4096]{2,1,0:T(8,128)(2,1)}, u32[]{:S(2)}) copy-start(bf16[1,352,4096]{2,1,0:T(8,128)(2,1)} %param.29) | copy-start | bytes 8650756
  0.7 5.3 %copy-start.5 = (pred[8]{0:T(512)(128)(4,1)}, pred[8]{0:T(512)(128)(4,1)S(1)}, u32[]{:S(2)}) copy-start(pred[8]{0:T(512)(128)(4,1)S(1)} %iota_compare_fusion.4) | copy-start | bytes 28
  13.6 11.7 %copy-start.1 = (bf16[32,4096]{1,0:T(8,128)(2,1)S(1)}, bf16[32,4096]{1,0:T(8,128)(2,1)}, u32[]{:S(2)}) copy-start(bf16[32,4096]{1,0:T(8,128)(2,1)} %param.23) | copy-start | bytes 786436
  22.4 58.5 %copy-start.4 = (f32[256]{0:T(256)S(1)}, f32[256]{0:T(256)}, u32[]{:S(2)}) copy-start(f32[256]{0:T(256)} %param.21) | copy-start | bytes 3076
  23.8 57.1 %copy-start.2 = (bf16[128,256]{0,1:T(8,128)(2,1)S(1)}, bf16[128,256]{0,1:T(8,128)(2,1)}, u32[]{:S(2)}) copy-start(bf16[128,256]{0,1:T(8,128)(2,1)} %copy.107) | copy-start | bytes 196612
  99.0 43.2 %copy-start.3 = (f32[32,128]{1,0:T(8,128)S(1)}, f32[32,128]{1,0:T(8,128)}, u32[]{:S(2)}) copy-start(f32[32,128]{1,0:T(8,128)} %select_reduce_fusion.1) | copy-start | bytes 49156

commit v2 on v1

v2 whole, which is shorter than its diff:
```python
import functools

import jax
import jax.numpy as jnp
from jax import lax
from jax.experimental import pallas as pl
from jax.experimental.pallas import tpu as pltpu
from jax.sharding import PartitionSpec as P

TOP = 2
SPAN = 64
MESH = pl.DeviceIdType.MESH


epsilon = 1e-06
highest = lax.Precision.HIGHEST


def visiting_order(count):
    return sorted(range(1, count), key=lambda k: abs(k - count // 2)) + [0]


def greet(me, tp, ep_count, tp_count, wait=True):
    pairs = tp_count // 2
    pair, side = tp // 2, tp % 2
    barrier = pltpu.get_barrier_semaphore()
    for k in range(1, ep_count):
        pl.semaphore_signal(
            barrier,
            inc=1,
            device_id={"ep": lax.rem(me + k, ep_count), "tp": tp},
            device_id_type=MESH,
        )
    for j in range(1, pairs):
        pl.semaphore_signal(
            barrier,
            inc=1,
            device_id={"ep": me, "tp": lax.rem(pair + j, pairs) * 2 + side},
            device_id_type=MESH,
        )
    pl.semaphore_signal(
        barrier, inc=1, device_id={"ep": me, "tp": pair * 2 + 1 - side}, device_id_type=MESH
    )
    if wait:
        pl.semaphore_wait(barrier, ep_count + pairs - 1)


def product(left, right, left_axis, right_axis, precision=None):
    return lax.dot_general(
        left,
        right,
        (((left_axis,), (right_axis,)), ((), ())),
        precision=precision,
        preferred_element_type=jnp.float32,
    )


def iota(shape, axis):
    return lax.broadcasted_iota(jnp.int32, shape, axis)


def dispatch_kernel(
    ep_count,
    tp_count,
    query_ref,
    forget_ref,
    value_ref,
    opening_ref,
    margin_ref,
    surge_ref,
    head_gain_ref,
    tokens_ref,
    gain_ref,
    routes_ref,
    logits_ref,
    gate_hbm,
    up_hbm,
    hidden_b_ref,
    hidden_a_ref,
    weights_ref,
    slots,
    piece,
    gate,
    up,
    lifted_ref,
    local_ref,
    window,
    window_total,
    before,
    before_total,
    outgoing,
    incoming,
    load,
    sa,
    ra,
    sy,
    ry,
    sc,
    rc,
    ss,
    rs,
):
    wide = jnp.float32
    me, tp = lax.axis_index("ep"), lax.axis_index("tp")
    pairs = tp_count // 2
    pair, side = tp // 2, tp % 2
    other = pair * 2 + 1 - side
    order = visiting_order(ep_count)
    heads, seq_len = surge_ref.shape
    key_width = query_ref.shape[1] // heads
    value_width = value_ref.shape[1] // heads
    tok_rows = tokens_ref.shape[0]
    capacity = slots.shape[1]
    slot_count = ep_count * capacity
    steps = outgoing.shape[0]

    greet(me, tp, ep_count, tp_count, wait=False)
    fetch = [
        pltpu.make_async_copy(gate_hbm, gate, load.at[0]),
        pltpu.make_async_copy(up_hbm, up, load.at[1]),
    ]
    for copy in fetch:
        copy.start()

    def remote(src, dst, send, recv, ep, to):
        return pltpu.make_async_remote_copy(
            src_ref=src,
            dst_ref=dst,
            send_sem=send,
            recv_sem=recv,
            device_id={"ep": ep, "tp": to},
            device_id_type=MESH,
        )

    def exchange(k):
        to = lax.rem(me + k, ep_count)
        return remote(slots.at[to], piece.at[tp, me], sa.at[k], ra.at[k], to, tp)

    def source(k):
        return lax.rem(me + ep_count - k, ep_count)

    def own_block(k):
        return slots.at[me] if k == 0 else piece.at[tp, source(k)]

    def across(k, j):
        to = lax.rem(pair + j, pairs) * 2 + side
        return remote(own_block(k), piece.at[tp, source(k)], sy.at[j, k], ry.at[j, k], me, to)

    def beside(k, j):
        block = lax.rem(pair + pairs - j, pairs) * 2 + side
        src = own_block(k) if j == 0 else piece.at[block, source(k)]
        return remote(src, piece.at[block, source(k)], sc.at[j, k], rc.at[j, k], me, other)

    def pass_on(k):
        for j in range(1, pairs):
            across(k, j).start()
        beside(k, 0).start()

    rows = tokens_ref[...].astype(wide)
    normed = (
        rows * lax.rsqrt(jnp.mean(rows * rows, axis=-1, keepdims=True) + epsilon) * gain_ref[...]
    ).astype(jnp.bfloat16)
    routes = routes_ref[pl.ds(pl.multiple_of(tp * tok_rows, tok_rows), tok_rows), :]
    named = [routes[:, i : i + 1] for i in range(TOP)]
    experts = iota((tok_rows, ep_count), 1)
    tables = [(column == experts).astype(wide) for column in named]
    strict = (iota((tok_rows, tok_rows), 0) > iota((tok_rows, tok_rows), 1)).astype(wide)
    earlier = product(strict, sum(tables), 1, 0, highest)
    places = [jnp.sum(earlier * table, axis=1, keepdims=True) for table in tables]
    spots = [
        column * capacity + place.astype(jnp.int32) for column, place in zip(named, places)
    ]
    for number, k in enumerate(order):
        to = lax.rem(me + k, ep_count)
        wanted = iota((tok_rows, capacity), 1) + to * capacity
        chooser = sum((spot == wanted).astype(wide) for spot in spots).astype(jnp.bfloat16)
        slots[to] = product(chooser, normed, 0, 0).astype(jnp.bfloat16)
        if number == 0:
            pl.semaphore_wait(pltpu.get_barrier_semaphore(), ep_count + pairs - 1)
        if k:
            exchange(k).start()
    pass_on(0)
    piece[tp, me] = slots[me]

    at, since = iota((seq_len, seq_len), 0), iota((seq_len, seq_len), 1)
    shut = jax.nn.sigmoid(-forget_ref[...].astype(wide)) * margin_ref[...]
    logarithm = jnp.log1p(-shut)
    within = ((at >= since) & (at // SPAN == since // SPAN)).astype(wide)
    running_all = product(within, logarithm, 1, 0, highest)
    triangle = iota((SPAN, SPAN), 0) >= iota((SPAN, SPAN), 1)
    for head in range(heads):
        keys = slice(head * key_width, (head + 1) * key_width)
        values = slice(head * value_width, (head + 1) * value_width)
        surges = jnp.sum(within * surge_ref[head : head + 1, :], axis=1, keepdims=True)
        running_head = running_all[:, keys] + surges
        state = jnp.zeros((value_width, key_width), wide)
        total = jnp.zeros((1, key_width), wide)
        for span in range(seq_len // SPAN):
            part = slice(span * SPAN, (span + 1) * SPAN)
            running = running_head[part]
            closing = running[SPAN - 1 : SPAN]
            inflow = shut[part, keys]
            value = value_ref[part, values].astype(wide)
            query = query_ref[part, keys].astype(wide)
            lifted = query * jnp.exp(running)
            scores = product(lifted, inflow * jnp.exp(-running), 1, 1, highest)
            scores = jnp.where(triangle, scores, 0.0)
            local = product(scores, value, 1, 0, highest)
            if span:
                local = local + product(lifted, state, 1, 1, highest)
            local_ref[part, values] = local
            lifted_ref[part, keys] = query * jnp.exp(running + total)
            fresh = product(value, inflow * jnp.exp(closing - running), 0, 0, highest)
            state = jnp.exp(closing) * state + fresh
            total = total + closing
        window[head] = state
        window_total[head] = total
    before[...] = jnp.zeros_like(before)
    before_total[...] = jnp.zeros_like(before_total)

    def state_copy(step):
        to = lax.rem(me + 2**step, ep_count)
        return remote(outgoing.at[step], incoming.at[step], ss.at[step], rs.at[step], to, tp)

    def send_window(step):
        for head in range(heads):
            outgoing[step, head, :value_width] = window[head].astype(jnp.bfloat16)
            total = window_total[head]
            coarse = total.astype(jnp.bfloat16).astype(wide)
            line = iota((16, key_width), 0)
            tail = jnp.where(line == 0, coarse, jnp.where(line == 1, total - coarse, 0.0))
            outgoing[step, head, value_width:] = tail.astype(jnp.bfloat16)

        @pl.when(me + 2**step < ep_count)
        def _():
            state_copy(step).start()

    def take_window(step):
        @pl.when(me >= 2**step)
        def _():
            state_copy(step).wait_recv()
            for head in range(heads):
                state = incoming[step, head, :value_width].astype(wide)
                total = jnp.sum(
                    incoming[step, head, value_width:].astype(wide), axis=0, keepdims=True
                )
                before[head] = jnp.exp(before_total[head]) * state + before[head]
                before_total[head] = before_total[head] + total
                window[head] = jnp.exp(window_total[head]) * state + window[head]
                window_total[head] = window_total[head] + total

    sequence = [0] + order[:-1]
    done = 0
    send_window(0)
    for position, k in enumerate(sequence):
        if k:
            exchange(k).wait_recv()
            pass_on(k)
        if position:
            last = sequence[position - 1]
            for j in range(1, pairs):
                across(last, j).wait_recv()
                beside(last, j).start()
        if position >= 2 and position % 2 == 0 and done < steps:
            take_window(done)
            done += 1
            if done < steps:
                send_window(done)
    while done < steps:
        take_window(done)
        done += 1
        if done < steps:
            send_window(done)
    for j in range(1, pairs):
        across(sequence[-1], j).wait_recv()
        beside(sequence[-1], j).start()

    for head in range(heads):
        keys = slice(head * key_width, (head + 1) * key_width)
        values = slice(head * value_width, (head + 1) * value_width)
        out = local_ref[:, values] + product(lifted_ref[:, keys], before[head], 1, 1, highest)
        out = out * lax.rsqrt(jnp.mean(out * out, axis=-1, keepdims=True) + epsilon)
        opening = opening_ref[:, values].astype(wide)
        hidden_a_ref[:, values] = (
            out * head_gain_ref[:, values] * (opening * jax.nn.sigmoid(opening))
        ).astype(jnp.bfloat16)
    logits = logits_ref[...]
    raised = jnp.exp(logits - jnp.max(logits, axis=-1, keepdims=True))
    share = raised / jnp.sum(raised, axis=-1, keepdims=True)
    numbers = iota((tok_rows, slot_count), 1)
    weights_ref[...] = sum(
        jnp.where(spot == numbers, share[:, i : i + 1], 0.0) for i, spot in enumerate(spots)
    )

    for k in sequence:
        for j in range(pairs):
            beside(k, j).wait_recv()
    for copy in fetch:
        copy.wait()

    def experts_of(block, carry):
        if capacity % 16:
            taken = jnp.concatenate([piece[block, e] for e in range(ep_count)], axis=0)
        else:
            taken = piece[block].reshape(slot_count, piece.shape[-1])
        left = product(taken, gate[...], 1, 0)
        right = product(taken, up[...], 1, 0)
        hidden_b_ref[block] = (left * jax.nn.sigmoid(left) * right).astype(jnp.bfloat16)
        return carry

    lax.fori_loop(0, tp_count, experts_of, 0)

    for k in range(1, ep_count):
        exchange(k).wait_send()
    for k in sequence:
        for j in range(pairs):
            if j:
                across(k, j).wait_send()
            beside(k, j).wait_send()
    for step in range(steps):

        @pl.when(me + 2**step < ep_count)
        def _(step=step):
            state_copy(step).wait_send()


def dispatch(small, gate, up, heads, capacity, ep_count, tp_count):
    pairs = tp_count // 2
    dma = pltpu.SemaphoreType.DMA
    vmem = pl.BlockSpec(memory_space=pltpu.VMEM)
    hbm = pl.BlockSpec(memory_space=pl.ANY)
    query, value, tokens = small[0], small[2], small[7]
    seq_len, keys = query.shape
    values = value.shape[1]
    tok_rows, width = tokens.shape
    key_width, value_width = keys // heads, values // heads
    steps = (ep_count - 1).bit_length()
    both = dma((pairs, ep_count))
    kind = jnp.bfloat16
    return pl.pallas_call(
        functools.partial(dispatch_kernel, ep_count, tp_count),
        out_shape=(
            jax.ShapeDtypeStruct((tp_count, ep_count * capacity, gate.shape[1]), kind),
            jax.ShapeDtypeStruct((seq_len, values), kind),
            jax.ShapeDtypeStruct((tok_rows, ep_count * capacity), jnp.float32),
        ),
        in_specs=[vmem] * len(small) + [hbm] * 2,
        out_specs=(vmem, vmem, vmem),
        scratch_shapes=[
            pltpu.VMEM((ep_count, capacity, width), kind),
            pltpu.VMEM((tp_count, ep_count, capacity, width), kind),
            pltpu.VMEM(gate.shape, kind),
            pltpu.VMEM(up.shape, kind),
            pltpu.VMEM((seq_len, keys), jnp.float32),
            pltpu.VMEM((seq_len, values), jnp.float32),
            pltpu.VMEM((heads, value_width, key_width), jnp.float32),
            pltpu.VMEM((heads, 1, key_width), jnp.float32),
            pltpu.VMEM((heads, value_width, key_width), jnp.float32),
            pltpu.VMEM((heads, 1, key_width), jnp.float32),
            pltpu.VMEM((steps, heads, value_width + 16, key_width), kind),
            pltpu.VMEM((steps, heads, value_width + 16, key_width), kind),
            dma((2,)),
            dma((ep_count,)),
            dma((ep_count,)),
            both,
            both,
            both,
            both,
            dma((steps,)),
            dma((steps,)),
        ],
        compiler_params=pltpu.CompilerParams(
            collective_id=0, has_side_effects=True, vmem_limit_bytes=60 << 20
        ),
    )(*small, gate, up)


def return_kernel(
    ep_count,
    tp_count,
    parts,
    mix,
    mixed,
    returned,
    cbuf,
    cmix,
    ysend,
    ysmix,
    ybuf,
    ymix,
    abuf,
    sc,
    rc,
    sy,
    ry,
    sa,
    ra,
):
    me, tp = lax.axis_index("ep"), lax.axis_index("tp")
    pairs = tp_count // 2
    pair, side = tp // 2, tp % 2
    other = pair * 2 + 1 - side
    order = visiting_order(ep_count)
    greet(me, tp, ep_count, tp_count)

    def remote(src, dst, send, recv, ep, to):
        return pltpu.make_async_remote_copy(
            src_ref=src,
            dst_ref=dst,
            send_sem=send,
            recv_sem=recv,
            device_id={"ep": ep, "tp": to},
            device_id_type=MESH,
        )

    def chunk(k):
        return lax.rem(me + k, ep_count)

    def toward(j):
        return lax.rem(pair + j, pairs)

    def beside(k, j):
        block = toward(j) * 2 + 1 - side
        if k == ep_count:
            return remote(mix.at[block], cmix.at[j], sc.at[j, k], rc.at[j, k], me, other)
        return remote(parts.at[block, chunk(k)], cbuf.at[j, k], sc.at[j, k], rc.at[j, k], me, other)

    def across(k, j):
        to = toward(j) * 2 + side
        if k == ep_count:
            return remote(ysmix.at[j], ymix.at[j], sy.at[j, k], ry.at[j, k], me, to)
        return remote(ysend.at[j, k], ybuf.at[j, k], sy.at[j, k], ry.at[j, k], me, to)

    def home(k):
        return remote(abuf.at[k], returned.at[me], sa.at[k], ra.at[k], chunk(k), tp)

    wide = jnp.float32
    everything = order + [ep_count]
    for k in everything:
        for j in list(range(1, pairs)) + [0]:
            beside(k, j).start()
    for k in everything:
        for j in range(1, pairs):
            beside(k, j).wait_recv()
            block = toward(j) * 2 + side
            if k == ep_count:
                ysmix[j] = (mix[block].astype(wide) + cmix[j].astype(wide)).astype(mix.dtype)
            else:
                ysend[j, k] = (
                    parts[block, chunk(k)].astype(wide) + cbuf[j, k].astype(wide)
                ).astype(parts.dtype)
            across(k, j).start()
    for k in everything:
        beside(k, 0).wait_recv()
        if k == ep_count:
            total = mix[tp].astype(wide) + cmix[0].astype(wide)
        else:
            total = parts[tp, chunk(k)].astype(wide) + cbuf[0, k].astype(wide)
        for j in range(1, pairs):
            across(k, j).wait_recv()
            total = total + (ymix[j] if k == ep_count else ybuf[j, k]).astype(wide)
        total = total.astype(parts.dtype)
        if k == ep_count:
            mixed[...] = total
        elif k == 0:
            returned[me] = total
        else:
            abuf[k] = total
            home(k).start()
    for k in everything:
        for j in range(pairs):
            beside(k, j).wait_send()
            if j:
                across(k, j).wait_send()
        if 0 < k < ep_count:
            home(k).wait()


def give_back(parts, mix, ep_count, tp_count):
    pairs = tp_count // 2
    dma = pltpu.SemaphoreType.DMA
    vmem = pl.BlockSpec(memory_space=pltpu.VMEM)
    chunks, rows = parts.shape[1:], mix.shape[1:]
    many = (pairs, ep_count + 1)
    kind = parts.dtype
    return pl.pallas_call(
        functools.partial(return_kernel, ep_count, tp_count),
        out_shape=(
            jax.ShapeDtypeStruct(rows, kind),
            jax.ShapeDtypeStruct(chunks, kind),
        ),
        in_specs=[vmem] * 2,
        out_specs=(vmem, vmem),
        scratch_shapes=[
            pltpu.VMEM((pairs,) + chunks, kind),
            pltpu.VMEM((pairs,) + rows, kind),
            pltpu.VMEM((pairs,) + chunks, kind),
            pltpu.VMEM((pairs,) + rows, kind),
            pltpu.VMEM((pairs,) + chunks, kind),
            pltpu.VMEM((pairs,) + rows, kind),
            pltpu.VMEM(chunks, kind),
            dma(many),
            dma(many),
            dma(many),
            dma(many),
            dma((ep_count,)),
            dma((ep_count,)),
        ],
        compiler_params=pltpu.CompilerParams(collective_id=1, has_side_effects=True),
    )(parts, mix)


def per_device(
    recurrence_query,
    forget_preactivation,
    recurrence_value,
    output_gate_preactivation,
    forget_margin,
    surge_log_decay,
    head_norm_gain,
    recurrence_output_matrix,
    second_micro_input,
    expert_norm_gain,
    routes,
    router_chosen_logits,
    expert_gate_matrix,
    expert_up_matrix,
    expert_down_matrix,
):
    number_of_heads = surge_log_decay.shape[0]
    seq_len = recurrence_query.shape[0]
    tp_count = lax.axis_size("tp")
    expert_count = lax.axis_size("ep")
    tok_rows, width = second_micro_input.shape
    capacity = 2 * tok_rows * TOP // expert_count
    small = (
        recurrence_query,
        forget_preactivation,
        recurrence_value,
        output_gate_preactivation,
        forget_margin[None, :],
        surge_log_decay,
        head_norm_gain[None, :],
        second_micro_input,
        expert_norm_gain[None, :],
        routes,
        router_chosen_logits,
    )
    hidden_b, hidden_a, weights = dispatch(
        small,
        expert_gate_matrix[0],
        expert_up_matrix[0],
        number_of_heads,
        capacity,
        expert_count,
        tp_count,
    )
    hidden_b = hidden_b.reshape(-1, hidden_b.shape[-1])
    mix_rows = seq_len // tp_count
    mix_parts = jnp.dot(
        hidden_a, recurrence_output_matrix, preferred_element_type=jnp.float32
    ).astype(jnp.bfloat16)
    expert_parts = jnp.dot(
        hidden_b, expert_down_matrix[0], preferred_element_type=jnp.float32
    ).astype(jnp.bfloat16)
    mixed, returned = give_back(
        expert_parts.reshape(tp_count, expert_count, capacity, width),
        mix_parts.reshape(tp_count, mix_rows, width),
        expert_count,
        tp_count,
    )
    moe_out = jnp.dot(
        weights, returned.reshape(-1, width).astype(jnp.float32), precision=highest
    )
    return (mixed, moe_out.astype(jnp.bfloat16))


def solution(mesh):
    return jax.shard_map(
        per_device,
        mesh=mesh,
        in_specs=(
            P("ep", "tp"),
            P("ep", "tp"),
            P("ep", "tp"),
            P("ep", "tp"),
            P("tp"),
            P("tp", "ep"),
            P("tp"),
            P("tp", None),
            P(("ep", "tp"), None),
            P(),
            P("ep", None),
            P(("ep", "tp"), None),
            P("ep", None, "tp"),
            P("ep", None, "tp"),
            P("ep", "tp", None),
        ),
        out_specs=(P(("ep", "tp"), None), P(("ep", "tp"), None)),
        check_vma=False,
    )
```

time: 147 us -> 118 us (0.80)
  matrix products: 26.4 us -> 9.86 us
  other arithmetic: 15.8 us -> 0 us
  Pallas kernels: 91.6 us -> 93.7 us
  local copies, waits for them, and re-layouts: 11.7 us -> 13.8 us
    dot_general x11 -> x0, matrix products: 11.6 us -> none  [the longest x1 5.7 us: expert_hidden(): jnp.dot(flat_rows, gate_local, preferred_element_type=jnp.float32)]
    unnamed x18 -> x11, local copies, waits for them, and re-layouts: 6.21 us -> 13.8 us
    reduce_sum x8 -> x0, other arithmetic: 5.71 us -> none  [the longest x1 1.39 us: per_device(): jnp.sum(survive[:, :, :, None] * states[:, :, :key_rows, :].astype(jnp.fl...]
    dot_general x1, matrix products: 9.17 us -> 4.28 us  [per_device(): jnp.dot(hidden_b, expert_down_matrix[0], preferred_element_type=jnp.float32)]
    pallas_call x1, Pallas kernels: 48.3 us -> 51.6 us  [dispatch(): pl.pallas_call(functools.partial(dispatch_kernel, ep_count, tp_count), ou...]
    transpose x5 -> x0, local copies, waits for them, and re-layouts: 2.87 us -> none  [the longest x3 1.94 us: heads_leading(): array.astype(jnp.float32).reshape(seq_len, number_of_heads, -1)]
    concatenate x1 -> x0, other arithmetic: 1.51 us -> none  [per_device(): jnp.concatenate([final_state.astype(jnp.bfloat16), jnp.swapaxes(jnp.stack...]
where the time goes in v2:
time: 118 us
  Pallas kernels  93.7 us (79%)
  local copies, waits for them, and re-layouts  13.8 us (12%)
  matrix products  9.86 us (8%)
    pallas_call x1, Pallas kernels, dispatch(): pl.pallas_call(functools.partial(dispatch_kernel, ep_count, tp_count), ou...  51.6 us
    pallas_call x1, Pallas kernels, give_back(): pl.pallas_call(functools.partial(return_kernel, ep_count, tp_count), out_...  42 us
    unnamed x11, local copies, waits for them, and re-layouts  13.8 us
    dot_general x1, matrix products, per_device(): jnp.dot(hidden_b, expert_down_matrix[0], preferred_element_type=jnp.float32)  4.28 us
    dot_general x1, matrix products, per_device(): jnp.dot(hidden_a, recurrence_output_matrix, preferred_element_type=jnp.fl...  3.11 us
    dot_general x1, matrix products, per_device(): jnp.dot(weights, returned.reshape(-1, width).astype(jnp.float32), precisi...  2.46 us

profile of v2, /device:TPU:0, one launch (start us, length us, event | category | flops | bytes accessed | tf_op | source)
XLA Modules:
  0.0 118.0 jit_solution(13712520791872677299)
XLA Ops:
  0.6 0.0 copy-start
  0.6 1.5 %copy.20.logits_ref = f32[32,2]{1,0:T(8,128)} copy(f32[32,2]{0,1:T(2,128)} %param.26) | data formatting | bytes 512 | tf_op args[11]
  2.2 1.4 %copy.19.routes_ref = s32[128,2]{1,0:T(8,128)} copy(s32[128,2]{0,1:T(2,128)} %param.25) | data formatting | bytes 2048 | tf_op args[10]
  3.6 4.6 %copy.17 = bf16[1,4096,352]{2,1,0:T(8,128)(2,1)} copy(bf16[1,4096,352]{1,2,0:T(8,128)(2,1)} %param.27) | data formatting | bytes 5767168 | tf_op args[12]
  8.2 4.6 %copy.18 = bf16[1,4096,352]{2,1,0:T(8,128)(2,1)} copy(bf16[1,4096,352]{1,2,0:T(8,128)(2,1)} %param.28) | data formatting | bytes 5767168 | tf_op args[13]
  12.8 51.6 %shard_map.158 = (bf16[4,128,352]{2,1,0:T(8,128)(2,1)}, bf16[128,256]{1,0:T(8,128)(2,1)}, f32[32,128]{1,0:T(8,128)}) custom-call(bf16[128,256]{1,0:T(8,128)(2,1)} %query_ref.1, bf16[128,256]{1,0:T(8,128)(2,1)} %forget_ref.1, bf16[128,256]{1,0:T(8,128)(2,1)} %value_ref.1, bf16[128,256]{1,0:T(8,128)(2,1)} %opening_ref.1, f32[1,256]{1,0:T(1,128)} %bitcast.23, ...), custom_call_target="tpu_custom_call" | custom-call | tf_op jit(solution)/shard_map/pallas_call | solution.py:340
  64.4 0.0 copy-start.2
  64.4 3.1 %convolution_convert_fusion.1 = bf16[128,4096]{1,0:T(8,128)(2,1)} fusion(bf16[128,256]{1,0:T(8,128)(2,1)} %get-tuple-element.8, bf16[256,4096]{1,0:T(8,128)(2,1)} %param.22), kind=kOutput, calls=%fused_computation.1 | convolution fusion | flops 268959744 | bytes 3211264 | tf_op jit(solution)/shard_map/dot_general | solution.py:560
  67.5 0.0 copy-done
  67.5 0.0 copy-done.2
  67.5 4.3 %convolution_convert_fusion = bf16[512,4096]{1,0:T(8,128)(2,1)} fusion(bf16[512,352]{1,0:T(8,128)(2,1)S(1)} %bitcast.25, bf16[1,352,4096]{2,1,0:T(8,128)(2,1)S(1)} %copy-done), kind=kOutput, calls=%fused_computation | convolution fusion | flops 1478492160 | bytes 7438336 | tf_op jit(solution)/shard_map/dot_general | solution.py:563
  71.8 0.0 copy-start.1
  71.8 42.0 %shard_map.159 = (bf16[32,4096]{1,0:T(8,128)(2,1)}, bf16[8,16,4096]{2,1,0:T(8,128)(2,1)}) custom-call(bf16[4,8,16,4096]{3,2,1,0:T(8,128)(2,1)} %bitcast.20, bf16[4,32,4096]{2,1,0:T(8,128)(2,1)} %bitcast.19), custom_call_target="tpu_custom_call" | custom-call | tf_op jit(solution)/shard_map/pallas_call | solution.py:486
  113.9 0.0 copy-done.1
  113.9 2.5 %convolution_convert_fusion.2 = bf16[32,4096]{1,0:T(8,128)(2,1)} fusion(f32[32,128]{1,0:T(8,128)S(1)} %copy-done.1, bf16[128,4096]{1,0:T(8,128)(2,1)} %bitcast.21), kind=kOutput, calls=%fused_computation.2 | convolution fusion | flops 201457664 | bytes 1327104 | tf_op jit(solution)/shard_map/dot_general | solution.py:572
  116.3 1.7 %copy.22 = bf16[32,4096]{1,0:T(8,128)(2,1)} copy(bf16[32,4096]{1,0:T(8,128)(2,1)} %get-tuple-element.14) | data formatting | bytes 524288
Async XLA Ops:
  0.6 66.9 %copy-start = (bf16[1,352,4096]{2,1,0:T(8,128)(2,1)S(1)}, bf16[1,352,4096]{2,1,0:T(8,128)(2,1)}, u32[]{:S(2)}) copy-start(bf16[1,352,4096]{2,1,0:T(8,128)(2,1)} %param.29) | copy-start | bytes 8650756
  64.4 3.1 %copy-start.2 = (bf16[4,128,352]{2,1,0:T(8,128)(2,1)S(1)}, bf16[4,128,352]{2,1,0:T(8,128)(2,1)}, u32[]{:S(2)}) copy-start(bf16[4,128,352]{2,1,0:T(8,128)(2,1)} %get-tuple-element.7) | copy-start | bytes 1081348
  71.8 42.0 %copy-start.1 = (f32[32,128]{1,0:T(8,128)S(1)}, f32[32,128]{1,0:T(8,128)}, u32[]{:S(2)}) copy-start(f32[32,128]{1,0:T(8,128)} %get-tuple-element.10) | copy-start | bytes 49156
